TPU v7x, 512 devices: a whole 4x4x16 slice. The times are simulated.
512 devices in a mesh: tp: 64 (over z, y), dp: 8 (over x, core).
Axes of the slice: x: 4, y: 4, z: 16, core: 2. Of those that a mesh axis runs over, the one named last changes fastest.
Arguments:
- resid: bfloat16 [256, 2048], P('dp', 'tp'), may hold values from -6 to 6
- norm_gain: float32 [2, 2048], replicated, may hold values from 0.1 to 1.9
- w_query: bfloat16 [2, 2048, 2048], P(None, 'dp', 'tp'), may hold values from -0.125 to 0.125
- w_forget: bfloat16 [2, 2048, 2048], P(None, 'dp', 'tp'), may hold values from -0.125 to 0.125
- w_value: bfloat16 [2, 2048, 16, 128], P(None, 'dp', None, 'tp'), may hold values from -0.125 to 0.125
- w_gate: bfloat16 [2, 2048, 16, 128], P(None, 'dp', None, 'tp'), may hold values from -0.125 to 0.125
- gate_floor: float32 [2, 2048], replicated, may hold values from 0 to 0.9
- states: float32 [2, 256, 16, 128, 128], P(None, 'dp', None, 'tp'), may hold values from -1 to 1
- out_gain: float32 [2, 16, 128], P(None, None, 'tp'), may hold values from 0.1 to 1.9
- w_out: bfloat16 [2, 16, 128, 2048], P(None, None, 'tp'), may hold values from -0.125 to 0.125
Outputs:
- new_resid: bfloat16 [256, 2048], P('dp', 'tp')
- new_states: float32 [2, 256, 16, 128, 128], P(None, 'dp', None, 'tp')
All inputs are finite; a program needn't handle non-finite values.
Results may differ from a plain program's by a relative error of at most 0.029.
Values may be sent and summed in bfloat16 or wider, within the bound.
A program may use at most 64 MiB of HBM per device.

v0:
```python
import jax
import jax.numpy as jnp
from jax import lax
from jax.sharding import PartitionSpec as P

BLOCKS = 2
epsilon = 1e-06


def sent_to_all(value, axis):
    length = lax.axis_size(axis)
    return lax.all_to_all(
        jnp.broadcast_to(value[None], (length, *value.shape)), axis, 0, 0, tiled=True
    )


def in_order(parts, dim):
    shape = list(parts.shape[1:])
    shape[dim] *= parts.shape[0]
    return jnp.moveaxis(parts, 0, dim).reshape(shape)


def gather_directly(value, axis, dim):
    parts = sent_to_all(value, axis)
    return in_order(parts, dim)


def in_one_piece(arrays, axis, dim, along):
    ends, at = ([], 0)
    for a in arrays[:-1]:
        at += a.shape[along]
        ends.append(at)
    both = jnp.concatenate(arrays, axis=along)
    return tuple(jnp.split(lax.all_gather(both, axis, axis=dim, tiled=True), ends, axis=along))


def rows_first(arrays, axis, dims):
    turned = [jnp.moveaxis(a, dim, 0) for a, dim in zip(arrays, dims)]
    both = jnp.concatenate([t.reshape(len(t), -1) for t in turned], axis=1)
    out, at, finished = (lax.all_gather(both, axis, axis=0, tiled=True), 0, [])
    for t, dim in zip(turned, dims):
        share = out[:, at : at + t[0].size].reshape(-1, *t.shape[1:])
        finished.append(jnp.moveaxis(share, 0, dim))
        at += t[0].size
    return tuple(finished)


def of_everyone(value, axis):
    everything = sent_to_all(value, axis)
    return jnp.sum(everything, axis=0)


def in_blocks(value, dim, length):
    before, after = (value.shape[:dim], value.shape[dim + 1 :])
    return jnp.moveaxis(value.reshape(*before, length, -1, *after), dim, 0)


def summed_on_arrival(value, axis, dim):
    parts = in_blocks(value, dim, lax.axis_size(axis))
    arrived = lax.all_to_all(parts, axis, split_axis=0, concat_axis=0, tiled=True)
    return arrived.sum(axis=0)


def shards(
    resid, norm_gain, w_query, w_forget, w_value, w_gate, gate_floor, states, out_gain, w_out
):
    residual = resid
    seq_local = resid.shape[0]
    heads = states.shape[2]
    slice_cols = states.shape[3]
    head_dim = states.shape[4]
    row_count = w_query.shape[1]
    new_list = []
    for layer in range(BLOCKS):
        gathered = gather_directly(residual, "tp", 1)
        resid_f32 = gathered.astype(jnp.float32)
        inv_rms = lax.rsqrt(jnp.mean(resid_f32 * resid_f32, axis=1, keepdims=True) + epsilon)
        scaled = (resid_f32 * norm_gain[layer]).astype(jnp.bfloat16)
        query_rows = w_query[layer]
        forget_rows = w_forget[layer]
        value_rows = w_value[layer].reshape(row_count, -1)
        gate_rows = w_gate[layer].reshape(row_count, -1)
        zero_sums = (
            jnp.zeros((seq_local, query_rows.shape[1]), jnp.float32),
            jnp.zeros((seq_local, forget_rows.shape[1]), jnp.float32),
            jnp.zeros((seq_local, value_rows.shape[1]), jnp.float32),
            jnp.zeros((seq_local, gate_rows.shape[1]), jnp.float32),
        )
        totals = zero_sums
        pieces = in_one_piece((query_rows, forget_rows, value_rows, gate_rows), "dp", 0, 1)
        segments = pieces[0].shape[0] // row_count
        for part_index in range(segments):
            columns = lax.dynamic_slice_in_dim(scaled, part_index * row_count, row_count, 1)
            lo_row = part_index * row_count
            totals = tuple(
                (
                    total
                    + lax.optimization_barrier(
                        jnp.dot(
                            columns,
                            segment[lo_row : lo_row + row_count],
                            preferred_element_type=jnp.float32,
                        ).astype(jnp.bfloat16)
                    ).astype(jnp.float32)
                    for total, segment in zip(totals, pieces)
                )
            )
        queries, forget_pre, values, gate_pre = [
            (summed * inv_rms).astype(jnp.bfloat16) for summed in totals
        ]
        query_all, forget_all = rows_first((queries, forget_pre), "tp", (1, 1))
        floor_now = gate_floor[layer]
        keep = floor_now + (1.0 - floor_now) * jax.nn.sigmoid(forget_all.astype(jnp.float32))
        keep = keep.reshape(seq_local, heads, head_dim)
        value_f32 = values.astype(jnp.float32).reshape(seq_local, heads, slice_cols)
        state_new = (
            keep[:, :, None, :] * states[layer]
            + (1.0 - keep)[:, :, None, :] * value_f32[:, :, :, None]
        )
        query_f32 = query_all.astype(jnp.float32).reshape(seq_local, heads, head_dim)
        readout = jnp.sum(query_f32[:, :, None, :] * state_new, axis=3)
        power_sum = of_everyone(jnp.sum(readout * readout, axis=2), "tp")
        mean_square = power_sum[..., None] / head_dim
        gate_f32 = gate_pre.astype(jnp.float32).reshape(seq_local, heads, slice_cols)
        normed = (
            readout * lax.rsqrt(mean_square + epsilon) * out_gain[layer] * jax.nn.silu(gate_f32)
        ).astype(jnp.bfloat16)
        flattened = normed.reshape(seq_local, heads * slice_cols)
        weight_out = w_out[layer].reshape(heads * slice_cols, -1)
        branch = summed_on_arrival(
            lax.dot_general(
                weight_out, flattened, (((0,), (1,)), ((), ())), preferred_element_type=jnp.float32
            ),
            "tp",
            0,
        )
        residual = (residual.astype(jnp.float32) + branch.T).astype(jnp.bfloat16)
        new_list.append(state_new)
    return (residual, jnp.stack(new_list))


def solution(mesh):
    return jax.shard_map(
        shards,
        mesh=mesh,
        in_specs=(
            P("dp", "tp"),
            P(),
            P(None, "dp", "tp"),
            P(None, "dp", "tp"),
            P(None, "dp", None, "tp"),
            P(None, "dp", None, "tp"),
            P(),
            P(None, "dp", None, "tp", None),
            P(None, None, "tp"),
            P(None, None, "tp", None),
        ),
        out_specs=(P("dp", "tp"), P(None, "dp", None, "tp", None)),
        check_vma=False,
    )
```

profile of v0, /device:TPU:2, one launch (start us, length us, event | category | flops | bytes accessed | tf_op | source)
XLA Modules:
  0.0 415.4 jit_solution(12405203772914550517)
XLA Ops:
  0.6 0.8 broadcast_in_dim.8
  1.4 1.1 reshape.98
  2.5 18.9 %all-to-all-start = ((bf16[64,2,512]{2,1,0:T(2,128)(2,1)}), bf16[64,2,512]{2,1,0:T(2,128)(2,1)S(1)}, u32[]{:S(2)}, u32[]{:S(2)}) async-start(bf16[64,2,512]{2,1,0:T(2,128)(2,1)} %reshape.98), calls=%async_computation | async-start | bytes 262144 | tf_op jit(solution)/shard_map/all_to_all | solution.py:12
  21.4 0.6 fusion.167
  22.1 0.6 fusion.165
  22.8 0.7 copy-done.15
  23.5 0.6 fusion.166
  24.4 0.5 copy-done.18
  24.9 0.6 slice_bitcast_fusion.2
  25.6 13.2 %all_gather.12 = bf16[2048,128]{0,1:T(8,128)(2,1)S(1)} all-gather(bf16[256,128]{0,1:T(8,128)(2,1)S(1)} %pad_maximum_fusion.1), channel_id=1, replica_groups=mesh['tp'=64,'dp'=8] {'dp'}, dimensions={0}, use_global_device_ids=true | all-gather | bytes 589824 | tf_op jit(solution)/shard_map/all_gather | solution.py:34
  38.7 0.6 fusion.168
  39.4 0.7 mul.316
  40.1 0.7 copy-done.25
  40.8 0.6 broadcast_subtract_fusion.2
  42.1 0.6 copy.86
  42.7 0.5 reshape.92
  43.4 0.7 convolution_convert_fusion.39
  44.4 0.7 convolution_convert_fusion.38
  45.4 0.7 convolution_convert_fusion.37
  46.4 0.7 convolution_convert_fusion.36
  47.3 0.7 convolution_convert_fusion.35
  50.8 101.3 %all_gather.13 = bf16[2048,64]{1,0:T(8,128)(2,1)S(1)} all-gather(bf16[32,64]{1,0:T(8,128)(2,1)S(1)} %copy.87), channel_id=1, replica_groups=mesh['tp'=64,'dp'=8] {'tp'}, dimensions={0}, use_global_device_ids=true | all-gather | bytes 266240 | tf_op jit(solution)/shard_map/all_gather | solution.py:40
  153.0 0.7 copy-done.3
  153.9 1.4 fusion.7
  155.5 0.9 reshape.100
  156.4 12.3 %all-to-all-start.1 = ((f32[64,1,512]{2,1,0:T(1,128)}), f32[64,1,512]{2,1,0:T(1,128)S(1)}, u32[]{:S(2)}, u32[]{:S(2)}) async-start(f32[64,1,512]{2,1,0:T(1,128)} %reshape.100), calls=%async_computation.1 | async-start | bytes 262144 | tf_op jit(solution)/shard_map/all_to_all | solution.py:12
  169.1 18.0 %all-to-all-done.1 = f32[64,1,512]{2,1,0:T(1,128)S(1)} async-done(((f32[64,1,512]{2,1,0:T(1,128)}), f32[64,1,512]{2,1,0:T(1,128)S(1)}, u32[]{:S(2)}, u32[]{:S(2)}) %all-to-all-start.1) | async-done | bytes 131104 | tf_op jit(solution)/shard_map/all_to_all | solution.py:12
  187.1 0.5 broadcast.158
  187.6 0.9 reduce.4
  190.6 0.6 copy.125
  191.2 0.5 reshape.102
  191.7 22.7 %all_to_all.30 = f32[64,1,1024]{2,1,0:T(1,128)S(1)} all-to-all(f32[64,1,1024]{2,1,0:T(1,128)S(1)} %reshape.102), channel_id=1, replica_groups=mesh['tp'=64,'dp'=8] {'tp'}, dimensions={0} | all-to-all | bytes 524288 | tf_op jit(solution)/shard_map/all_to_all | solution.py:60
  214.3 1.2 reduce.5
  216.0 0.6 copy-done.13
  216.7 1.1 reshape.104
  217.8 4.7 %all-to-all-start.3 = ((bf16[64,2,512]{2,1,0:T(2,128)(2,1)}), bf16[64,2,512]{2,1,0:T(2,128)(2,1)S(1)}, u32[]{:S(2)}, u32[]{:S(2)}) async-start(bf16[64,2,512]{2,1,0:T(2,128)(2,1)} %reshape.104), calls=%async_computation.3 | async-start | bytes 262144 | tf_op jit(solution)/shard_map/all_to_all | solution.py:12
  222.6 0.7 mul.349
  223.3 0.7 copy-done.10
  224.0 0.7 reshape_squeeze.23
  224.8 13.1 %all_gather.14 = bf16[2048,128]{0,1:T(8,128)(2,1)S(1)} all-gather(bf16[256,128]{0,1:T(8,128)(2,1)S(1)} %pad_maximum_fusion.2), channel_id=1, replica_groups=mesh['tp'=64,'dp'=8] {'dp'}, dimensions={0}, use_global_device_ids=true | all-gather | bytes 589824 | tf_op jit(solution)/shard_map/all_gather | solution.py:34
  237.9 0.8 all-to-all-done.3
  239.3 0.6 copy.100
  240.0 0.5 reshape.95
  244.9 100.7 %all_gather.15 = bf16[2048,64]{1,0:T(8,128)(2,1)S(1)} all-gather(bf16[32,64]{1,0:T(8,128)(2,1)S(1)} %copy.101), channel_id=1, replica_groups=mesh['tp'=64,'dp'=8] {'tp'}, dimensions={0}, use_global_device_ids=true | all-gather | bytes 266240 | tf_op jit(solution)/shard_map/all_gather | solution.py:40
  345.9 1.0 copy.102
  347.1 0.5 copy-done.16
  347.8 0.9 copy-done.6
  348.7 1.3 fusion.4
  350.3 0.9 reshape.106
  351.2 12.4 %all-to-all-start.4 = ((f32[64,1,512]{2,1,0:T(1,128)}), f32[64,1,512]{2,1,0:T(1,128)S(1)}, u32[]{:S(2)}, u32[]{:S(2)}) async-start(f32[64,1,512]{2,1,0:T(1,128)} %reshape.106), calls=%async_computation.4 | async-start | bytes 262144 | tf_op jit(solution)/shard_map/all_to_all | solution.py:12
  363.6 0.8 convolution_convert_fusion.2
  364.4 0.8 convolution_convert_fusion.1
  365.2 0.8 convolution_convert_fusion
  366.1 15.6 %all-to-all-done.4 = f32[64,1,512]{2,1,0:T(1,128)S(1)} async-done(((f32[64,1,512]{2,1,0:T(1,128)}), f32[64,1,512]{2,1,0:T(1,128)S(1)}, u32[]{:S(2)}, u32[]{:S(2)}) %all-to-all-start.4) | async-done | bytes 131104 | tf_op jit(solution)/shard_map/all_to_all | solution.py:12
  381.7 0.9 reduce.6
  383.4 0.6 copy-done.7
  384.6 1.6 copy.124
  386.2 2.4 reshape.108
  388.6 5.9 %all-to-all-start.5 = ((f32[64,1,1024]{2,1,0:T(1,128)}), f32[64,1,1024]{2,1,0:T(1,128)S(1)}, u32[]{:S(2)}, u32[]{:S(2)}) async-start(f32[64,1,1024]{2,1,0:T(1,128)} %reshape.108), calls=%async_computation.5 | async-start | bytes 524288 | tf_op jit(solution)/shard_map/all_to_all | solution.py:60
  394.5 1.4 multiply_add_fusion.1
  395.9 1.5 pad_maximum_fusion
  397.4 15.7 %all-to-all-done.5 = f32[64,1,1024]{2,1,0:T(1,128)S(1)} async-done(((f32[64,1,1024]{2,1,0:T(1,128)}), f32[64,1,1024]{2,1,0:T(1,128)S(1)}, u32[]{:S(2)}, u32[]{:S(2)}) %all-to-all-start.5) | async-done | bytes 262176 | tf_op jit(solution)/shard_map/all_to_all | solution.py:60
  413.1 1.2 reduce.7
  414.8 0.6 fusion.80
  (187 shorter events, 17.1 us)
Async XLA Ops:
  1.4 20.0 %copy-start.26 = (f32[2,2048]{1,0:T(2,128)S(1)}, f32[2,2048]{1,0:T(2,128)}, u32[]{:S(2)}) copy-start(f32[2,2048]{1,0:T(2,128)} %param.11) | copy-start | bytes 49156
  2.5 21.7 %copy-start.8 = (bf16[2,16,2,2048]{3,2,1,0:T(2,128)(2,1)S(1)}, bf16[2,16,2,2048]{3,2,1,0:T(2,128)(2,1)}, u32[]{:S(2)}) copy-start(bf16[2,16,2,2048]{3,2,1,0:T(2,128)(2,1)} %param.19) | copy-start | bytes 786436
  2.5 38.9 %all-to-all-start = ((bf16[64,2,512]{2,1,0:T(2,128)(2,1)}), bf16[64,2,512]{2,1,0:T(2,128)(2,1)S(1)}, u32[]{:S(2)}, u32[]{:S(2)}) async-start(bf16[64,2,512]{2,1,0:T(2,128)(2,1)} %reshape.98), calls=%async_computation | async-start | bytes 262144 | tf_op jit(solution)/shard_map/all_to_all | solution.py:12
  21.4 0.8 copy-start.14
  22.8 0.8 copy-start.15
  24.2 0.8 copy-start.18
  24.2 0.8 copy-start.19
  25.6 13.2 %copy-start.30 = (f32[2,16,2]{1,2,0:T(2,128)S(1)}, f32[2,16,2]{1,2,0:T(2,128)}, u32[]{:S(2)}) copy-start(f32[2,16,2]{1,2,0:T(2,128)} %param.18) | copy-start | bytes 772
  40.1 0.7 copy-start.25
  49.8 0.6 copy-start.27
  50.8 102.2 %copy-start.1 = (f32[32,16,2]{2,1,0:T(8,128)}, f32[32,16,2]{2,1,0:T(8,128)S(1)}, u32[]{:S(2)}) copy-start(f32[32,16,2]{2,1,0:T(8,128)S(1)} %copy.91) | copy-start | bytes 12292
  152.6 1.2 copy-start
  153.0 0.7 copy-start.3
  156.4 30.7 %all-to-all-start.1 = ((f32[64,1,512]{2,1,0:T(1,128)}), f32[64,1,512]{2,1,0:T(1,128)S(1)}, u32[]{:S(2)}, u32[]{:S(2)}) async-start(f32[64,1,512]{2,1,0:T(1,128)} %reshape.100), calls=%async_computation.1 | async-start | bytes 262144 | tf_op jit(solution)/shard_map/all_to_all | solution.py:12
  189.0 0.7 copy-start.24
  189.0 0.7 copy-start.28
  189.0 0.7 copy-start.32
  189.2 0.7 copy-start.20
  189.2 0.7 copy-start.21
  189.2 0.7 copy-start.22
  189.2 0.7 copy-start.23
  215.9 0.7 copy-start.13
  216.7 5.8 %copy-start.29 = (f32[1,16,2]{1,2,0:T(2,128)S(1)}, f32[1,16,2]{1,2,0:T(2,128)}, u32[]{:S(2)}) copy-start(f32[1,16,2]{1,2,0:T(2,128)} %get-tuple-element.24) | copy-start | bytes 388
  217.8 20.9 %all-to-all-start.3 = ((bf16[64,2,512]{2,1,0:T(2,128)(2,1)}), bf16[64,2,512]{2,1,0:T(2,128)(2,1)S(1)}, u32[]{:S(2)}, u32[]{:S(2)}) async-start(bf16[64,2,512]{2,1,0:T(2,128)(2,1)} %reshape.104), calls=%async_computation.3 | async-start | bytes 262144 | tf_op jit(solution)/shard_map/all_to_all | solution.py:12
  222.5 0.8 copy-start.9
  223.3 0.7 copy-start.10
  224.0 0.7 copy-start.11
  224.0 0.7 copy-start.12
  237.9 6.4 %copy-start.5 = (bf16[2048,128]{0,1:T(8,128)(2,1)}, bf16[2048,128]{0,1:T(8,128)(2,1)S(1)}, u32[]{:S(2)}) copy-start(bf16[2048,128]{0,1:T(8,128)(2,1)S(1)} %all_gather.14) | copy-start | bytes 1572868
  240.0 0.7 copy-start.17
  346.9 0.7 copy-start.16
  347.7 1.0 copy-start.6
  351.2 30.5 %all-to-all-start.4 = ((f32[64,1,512]{2,1,0:T(1,128)}), f32[64,1,512]{2,1,0:T(1,128)S(1)}, u32[]{:S(2)}, u32[]{:S(2)}) async-start(f32[64,1,512]{2,1,0:T(1,128)} %reshape.106), calls=%async_computation.4 | async-start | bytes 262144 | tf_op jit(solution)/shard_map/all_to_all | solution.py:12
  383.1 0.9 copy-start.7
  383.3 0.7 copy-start.31
  388.6 5.9 %copy-start.2 = (f32[32,16,2]{2,1,0:T(8,128)S(1)}, f32[32,16,2]{2,1,0:T(8,128)}, u32[]{:S(2)}) copy-start(f32[32,16,2]{2,1,0:T(8,128)} %copy-done.1) | copy-start | bytes 12292
  388.6 5.9 %copy-start.4 = (f32[32,16,128]{2,1,0:T(8,128)S(1)}, f32[32,16,128]{2,1,0:T(8,128)}, u32[]{:S(2)}) copy-start(f32[32,16,128]{2,1,0:T(8,128)} %copy-done.3) | copy-start | bytes 786436
  388.6 24.5 %all-to-all-start.5 = ((f32[64,1,1024]{2,1,0:T(1,128)}), f32[64,1,1024]{2,1,0:T(1,128)S(1)}, u32[]{:S(2)}, u32[]{:S(2)}) async-start(f32[64,1,1024]{2,1,0:T(1,128)} %reshape.108), calls=%async_computation.5 | async-start | bytes 524288 | tf_op jit(solution)/shard_map/all_to_all | solution.py:60
where the time goes:
time: 417 us; the launch traced here: 415 us
  blocking collectives  251 us (60%)
  starting transfers between devices  54.2 us (13%)
  waiting for transfers between devices  50 us (12%)
  local copies, waits for them, and re-layouts  31.6 us (8%)
  other arithmetic  13.7 us (3%)
  matrix products  13.7 us (3%)
    all_gather x2, blocking collectives, rows_first(): out, at, finished = (lax.all_gather(both, axis, axis=0, tiled=True), 0, [])  202 us
    all_to_all x4, starting transfers between devices, sent_to_all(): lax.all_to_all(jnp.broadcast_to(value[None], (length, *value.shape)), axi...  48.3 us
    all_to_all x4, waiting for transfers between devices, sent_to_all(): lax.all_to_all(jnp.broadcast_to(value[None], (length, *value.shape)), axi...  34.3 us
    all_gather x2, blocking collectives, in_one_piece(): lax.all_gather(both, axis, axis=dim, tiled=True)  26.3 us
    all_to_all x1, blocking collectives, summed_on_arrival(): lax.all_to_all(parts, axis, split_axis=0, concat_axis=0, tiled=True)  22.7 us
    unnamed x84, local copies, waits for them, and re-layouts  16.5 us
    all_to_all x1, waiting for transfers between devices, summed_on_arrival(): lax.all_to_all(parts, axis, split_axis=0, concat_axis=0, tiled=True)  15.7 us
    dot_general x64, matrix products, shards(): jnp.dot(columns, segment[lo_row:lo_row + row_count], preferred_element_ty...  13.2 us
  transfers between devices with their start and end apart: 5, of which 4 were waited for; matrix products, arithmetic and copies ran while one was open for 3% of the time, Pallas kernels for 0%

commit v1 on v0

--- a/solution.py
+++ b/solution.py
@@ -37,7 +37,19 @@
 def rows_first(arrays, axis, dims):
     turned = [jnp.moveaxis(a, dim, 0) for a, dim in zip(arrays, dims)]
     both = jnp.concatenate([t.reshape(len(t), -1) for t in turned], axis=1)
-    out, at, finished = (lax.all_gather(both, axis, axis=0, tiled=True), 0, [])
+    out, at, finished = (
+        jnp.concatenate(
+            lax.all_to_all(
+                jnp.stack([both for _ in range(lax.axis_size(axis))], axis=0),
+                axis_name=axis,
+                split_axis=0,
+                concat_axis=0,
+            ),
+            axis=0,
+        ),
+        0,
+        [],
+    )
     for t, dim in zip(turned, dims):
         share = out[:, at : at + t[0].size].reshape(-1, *t.shape[1:])
         finished.append(jnp.moveaxis(share, 0, dim))

time: 417 us -> 278 us (0.67)
  blocking collectives: 251 us -> 52.3 us
  waiting for transfers between devices: 50 us -> 89.6 us
  starting transfers between devices: 54.2 us -> 67.5 us
    all_gather x2 -> x0, blocking collectives: 202 us -> none  [rows_first(): out, at, finished = (lax.all_gather(both, axis, axis=0, tiled=True), 0, [])]
    all_to_all x0 -> x2, waiting for transfers between devices: none -> 38.6 us  [rows_first(): lax.all_to_all(jnp.stack([both for _ in range(lax.axis_size(axis))], axis...]
    all_to_all x0 -> x2, starting transfers between devices: none -> 29.2 us  [rows_first(): lax.all_to_all(jnp.stack([both for _ in range(lax.axis_size(axis))], axis...]
    all_to_all x4, starting transfers between devices: 48.3 us -> 33.6 us  [sent_to_all(): lax.all_to_all(jnp.broadcast_to(value[None], (length, *value.shape)), axi...]
    unnamed x84 -> x104, local copies, waits for them, and re-layouts: 16.5 us -> 19.9 us
  transfers between devices with their start and end apart: 5 -> 7, of which waited for: 4 -> 6; matrix products, arithmetic and copies ran while one was open for 3% -> 7% of each run, Pallas kernels for 0% -> 0%
where the time goes in v1:
time: 278 us; the launch traced here: 276 us
  waiting for transfers between devices  89.6 us (32%)
  starting transfers between devices  67.5 us (24%)
  blocking collectives  52.3 us (19%)
  local copies, waits for them, and re-layouts  34.4 us (12%)
  matrix products  16.6 us (6%)
  other arithmetic  14.5 us (5%)
    all_to_all x2, waiting for transfers between devices, rows_first(): lax.all_to_all(jnp.stack([both for _ in range(lax.axis_size(axis))], axis...  38.6 us
    all_to_all x4, starting transfers between devices, sent_to_all(): lax.all_to_all(jnp.broadcast_to(value[None], (length, *value.shape)), axi...  33.6 us
    all_to_all x4, waiting for transfers between devices, sent_to_all(): lax.all_to_all(jnp.broadcast_to(value[None], (length, *value.shape)), axi...  32.1 us
    all_to_all x2, starting transfers between devices, rows_first(): lax.all_to_all(jnp.stack([both for _ in range(lax.axis_size(axis))], axis...  29.2 us
    all_gather x2, blocking collectives, in_one_piece(): lax.all_gather(both, axis, axis=dim, tiled=True)  26.3 us
    all_to_all x1, blocking collectives, summed_on_arrival(): lax.all_to_all(parts, axis, split_axis=0, concat_axis=0, tiled=True)  26 us
    unnamed x104, local copies, waits for them, and re-layouts  19.9 us
    all_to_all x1, waiting for transfers between devices, summed_on_arrival(): lax.all_to_all(parts, axis, split_axis=0, concat_axis=0, tiled=True)  18.8 us
  transfers between devices with their start and end apart: 7, of which 6 were waited for; matrix products, arithmetic and copies ran while one was open for 7% of the time, Pallas kernels for 0%

profile of v1, /device:TPU:2, one launch (start us, length us, event | category | flops | bytes accessed | tf_op | source)
XLA Modules:
  0.0 276.3 jit_solution(3779268150164554865)
XLA Ops:
  0.6 0.8 broadcast_in_dim.8
  1.4 1.1 reshape.110
  2.5 18.9 %all-to-all-start = ((bf16[64,2,512]{2,1,0:T(2,128)(2,1)}), bf16[64,2,512]{2,1,0:T(2,128)(2,1)S(1)}, u32[]{:S(2)}, u32[]{:S(2)}) async-start(bf16[64,2,512]{2,1,0:T(2,128)(2,1)} %reshape.110), calls=%async_computation | async-start | bytes 262144 | tf_op jit(solution)/shard_map/all_to_all | solution.py:12
  21.4 0.6 fusion.167
  22.1 0.6 fusion.165
  22.8 0.7 copy-done.15
  23.5 0.6 fusion.166
  24.9 0.6 slice_bitcast_fusion.2
  25.6 13.2 %all_gather.6 = bf16[2048,128]{0,1:T(8,128)(2,1)S(1)} all-gather(bf16[256,128]{0,1:T(8,128)(2,1)S(1)} %pad_maximum_fusion.1), channel_id=1, replica_groups=mesh['tp'=64,'dp'=8] {'dp'}, dimensions={0}, use_global_device_ids=true | all-gather | bytes 589824 | tf_op jit(solution)/shard_map/all_gather | solution.py:34
  39.4 0.7 mul.316
  40.1 0.7 copy-done.31
  40.8 0.6 broadcast_subtract_fusion.2
  42.1 0.6 copy.98
  47.3 1.0 reshape.112
  48.3 15.1 %all-to-all-start.1 = ((bf16[64,2,1024]{2,1,0:T(2,128)(2,1)}), bf16[64,2,1024]{2,1,0:T(2,128)(2,1)S(1)}, u32[]{:S(2)}, u32[]{:S(2)}) async-start(bf16[64,2,1024]{2,1,0:T(2,128)(2,1)} %reshape.112), calls=%async_computation.1 | async-start | bytes 524288 | tf_op jit(solution)/shard_map/all_to_all | solution.py:42
  63.4 0.7 convolution_convert_fusion.39
  64.2 0.7 convolution_convert_fusion.38
  64.9 0.7 convolution_convert_fusion.37
  65.6 0.7 convolution_convert_fusion.36
  66.3 0.7 convolution_convert_fusion.35
  67.0 19.4 %all-to-all-done.1 = bf16[64,2,1024]{2,1,0:T(2,128)(2,1)S(1)} async-done(((bf16[64,2,1024]{2,1,0:T(2,128)(2,1)}), bf16[64,2,1024]{2,1,0:T(2,128)(2,1)S(1)}, u32[]{:S(2)}, u32[]{:S(2)}) %all-to-all-start.1) | async-done | bytes 262176 | tf_op jit(solution)/shard_map/all_to_all | solution.py:42
  88.3 0.7 copy-done.3
  89.0 1.4 fusion.7
  90.6 0.9 reshape.114
  91.5 5.1 %all-to-all-start.2 = ((f32[64,1,512]{2,1,0:T(1,128)}), f32[64,1,512]{2,1,0:T(1,128)S(1)}, u32[]{:S(2)}, u32[]{:S(2)}) async-start(f32[64,1,512]{2,1,0:T(1,128)} %reshape.114), calls=%async_computation.2 | async-start | bytes 262144 | tf_op jit(solution)/shard_map/all_to_all | solution.py:12
  96.9 16.5 %all-to-all-done.2 = f32[64,1,512]{2,1,0:T(1,128)S(1)} async-done(((f32[64,1,512]{2,1,0:T(1,128)}), f32[64,1,512]{2,1,0:T(1,128)S(1)}, u32[]{:S(2)}, u32[]{:S(2)}) %all-to-all-start.2) | async-done | bytes 131104 | tf_op jit(solution)/shard_map/all_to_all | solution.py:12
  114.0 0.9 reduce.4
  117.0 0.6 copy.137
  118.0 26.0 %all_to_all.40 = f32[64,1,1024]{2,1,0:T(1,128)S(1)} all-to-all(f32[64,1,1024]{2,1,0:T(1,128)S(1)} %reshape.116), channel_id=1, replica_groups=mesh['tp'=64,'dp'=8] {'tp'}, dimensions={0} | all-to-all | bytes 524288 | tf_op jit(solution)/shard_map/all_to_all | solution.py:72
  144.1 1.2 reduce.5
  146.5 1.1 reshape.118
  147.5 4.8 %all-to-all-start.4 = ((bf16[64,2,512]{2,1,0:T(2,128)(2,1)}), bf16[64,2,512]{2,1,0:T(2,128)(2,1)S(1)}, u32[]{:S(2)}, u32[]{:S(2)}) async-start(bf16[64,2,512]{2,1,0:T(2,128)(2,1)} %reshape.118), calls=%async_computation.4 | async-start | bytes 262144 | tf_op jit(solution)/shard_map/all_to_all | solution.py:12
  152.4 0.6 mul.349
  153.1 0.7 copy-done.10
  153.8 0.7 reshape_squeeze.23
  154.5 13.1 %all_gather.7 = bf16[2048,128]{0,1:T(8,128)(2,1)S(1)} all-gather(bf16[256,128]{0,1:T(8,128)(2,1)S(1)} %pad_maximum_fusion.2), channel_id=1, replica_groups=mesh['tp'=64,'dp'=8] {'dp'}, dimensions={0}, use_global_device_ids=true | all-gather | bytes 589824 | tf_op jit(solution)/shard_map/all_gather | solution.py:34
  167.6 1.2 all-to-all-done.4
  169.5 0.6 copy.112
  175.0 1.0 reshape.120
  176.0 14.1 %all-to-all-start.5 = ((bf16[64,2,1024]{2,1,0:T(2,128)(2,1)}), bf16[64,2,1024]{2,1,0:T(2,128)(2,1)S(1)}, u32[]{:S(2)}, u32[]{:S(2)}) async-start(bf16[64,2,1024]{2,1,0:T(2,128)(2,1)} %reshape.120), calls=%async_computation.5 | async-start | bytes 524288 | tf_op jit(solution)/shard_map/all_to_all | solution.py:42
  190.1 0.7 convolution_convert_fusion.7
  190.8 0.7 convolution_convert_fusion.6
  191.6 0.7 convolution_convert_fusion.5
  192.3 0.7 convolution_convert_fusion.4
  193.0 0.7 convolution_convert_fusion.3
  193.7 19.2 %all-to-all-done.5 = bf16[64,2,1024]{2,1,0:T(2,128)(2,1)S(1)} async-done(((bf16[64,2,1024]{2,1,0:T(2,128)(2,1)}), bf16[64,2,1024]{2,1,0:T(2,128)(2,1)S(1)}, u32[]{:S(2)}, u32[]{:S(2)}) %all-to-all-start.5) | async-done | bytes 262176 | tf_op jit(solution)/shard_map/all_to_all | solution.py:42
  213.3 1.0 slice_convert_fusion
  214.6 0.7 copy-done.5
  216.2 1.3 fusion.4
  217.8 0.9 reshape.122
  218.7 4.9 %all-to-all-start.6 = ((f32[64,1,512]{2,1,0:T(1,128)}), f32[64,1,512]{2,1,0:T(1,128)S(1)}, u32[]{:S(2)}, u32[]{:S(2)}) async-start(f32[64,1,512]{2,1,0:T(1,128)} %reshape.122), calls=%async_computation.6 | async-start | bytes 262144 | tf_op jit(solution)/shard_map/all_to_all | solution.py:12
  223.6 0.8 convolution_convert_fusion.2
  224.4 0.8 convolution_convert_fusion.1
  225.3 0.8 convolution_convert_fusion
  226.1 14.5 %all-to-all-done.6 = f32[64,1,512]{2,1,0:T(1,128)S(1)} async-done(((f32[64,1,512]{2,1,0:T(1,128)}), f32[64,1,512]{2,1,0:T(1,128)S(1)}, u32[]{:S(2)}, u32[]{:S(2)}) %all-to-all-start.6) | async-done | bytes 131104 | tf_op jit(solution)/shard_map/all_to_all | solution.py:12
  240.6 0.9 reduce.6
  243.6 1.6 copy.136
  245.2 2.4 reshape.124
  247.6 4.7 %all-to-all-start.7 = ((f32[64,1,1024]{2,1,0:T(1,128)}), f32[64,1,1024]{2,1,0:T(1,128)S(1)}, u32[]{:S(2)}, u32[]{:S(2)}) async-start(f32[64,1,1024]{2,1,0:T(1,128)} %reshape.124), calls=%async_computation.7 | async-start | bytes 524288 | tf_op jit(solution)/shard_map/all_to_all | solution.py:72
  252.4 1.4 multiply_add_fusion.1
  253.8 1.5 pad_maximum_fusion
  255.3 18.8 %all-to-all-done.7 = f32[64,1,1024]{2,1,0:T(1,128)S(1)} async-done(((f32[64,1,1024]{2,1,0:T(1,128)}), f32[64,1,1024]{2,1,0:T(1,128)S(1)}, u32[]{:S(2)}, u32[]{:S(2)}) %all-to-all-start.7) | async-done | bytes 262176 | tf_op jit(solution)/shard_map/all_to_all | solution.py:72
  274.0 1.2 reduce.7
  275.7 0.6 fusion.80
  (211 shorter events, 23.1 us)
Async XLA Ops:
  1.4 20.0 %copy-start.32 = (f32[2,2048]{1,0:T(2,128)S(1)}, f32[2,2048]{1,0:T(2,128)}, u32[]{:S(2)}) copy-start(f32[2,2048]{1,0:T(2,128)} %param.11) | copy-start | bytes 49156
  2.5 21.7 %copy-start.8 = (bf16[2,16,2,2048]{3,2,1,0:T(2,128)(2,1)S(1)}, bf16[2,16,2,2048]{3,2,1,0:T(2,128)(2,1)}, u32[]{:S(2)}) copy-start(bf16[2,16,2,2048]{3,2,1,0:T(2,128)(2,1)} %param.19) | copy-start | bytes 786436
  2.5 38.9 %all-to-all-start = ((bf16[64,2,512]{2,1,0:T(2,128)(2,1)}), bf16[64,2,512]{2,1,0:T(2,128)(2,1)S(1)}, u32[]{:S(2)}, u32[]{:S(2)}) async-start(bf16[64,2,512]{2,1,0:T(2,128)(2,1)} %reshape.110), calls=%async_computation | async-start | bytes 262144 | tf_op jit(solution)/shard_map/all_to_all | solution.py:12
  21.4 0.8 copy-start.14
  22.8 0.8 copy-start.15
  24.2 0.8 copy-start.19
  24.2 0.8 copy-start.20
  25.6 13.2 %copy-start.38 = (f32[2,16,2]{1,2,0:T(2,128)S(1)}, f32[2,16,2]{1,2,0:T(2,128)}, u32[]{:S(2)}) copy-start(f32[2,16,2]{1,2,0:T(2,128)} %param.18) | copy-start | bytes 772
  40.1 0.7 copy-start.31
  46.3 0.6 copy-start.33
  47.2 41.0 %copy-start.1 = (f32[32,16,2]{2,1,0:T(8,128)}, f32[32,16,2]{2,1,0:T(8,128)S(1)}, u32[]{:S(2)}) copy-start(f32[32,16,2]{2,1,0:T(8,128)S(1)} %copy.103) | copy-start | bytes 12292
  48.3 38.1 %all-to-all-start.1 = ((bf16[64,2,1024]{2,1,0:T(2,128)(2,1)}), bf16[64,2,1024]{2,1,0:T(2,128)(2,1)S(1)}, u32[]{:S(2)}, u32[]{:S(2)}) async-start(bf16[64,2,1024]{2,1,0:T(2,128)(2,1)} %reshape.112), calls=%async_computation.1 | async-start | bytes 524288 | tf_op jit(solution)/shard_map/all_to_all | solution.py:42
  87.4 0.7 copy-start.18
  87.4 1.6 copy-start
  88.3 0.7 copy-start.3
  91.5 21.9 %all-to-all-start.2 = ((f32[64,1,512]{2,1,0:T(1,128)}), f32[64,1,512]{2,1,0:T(1,128)S(1)}, u32[]{:S(2)}, u32[]{:S(2)}) async-start(f32[64,1,512]{2,1,0:T(1,128)} %reshape.114), calls=%async_computation.2 | async-start | bytes 262144 | tf_op jit(solution)/shard_map/all_to_all | solution.py:12
  115.4 0.7 copy-start.25
  115.4 0.7 copy-start.34
  115.4 0.7 copy-start.40
  115.6 0.7 copy-start.21
  115.6 0.7 copy-start.22
  115.6 0.7 copy-start.23
  115.6 0.7 copy-start.24
  145.7 0.7 copy-start.13
  146.5 5.9 %copy-start.37 = (f32[1,16,2]{1,2,0:T(2,128)S(1)}, f32[1,16,2]{1,2,0:T(2,128)}, u32[]{:S(2)}) copy-start(f32[1,16,2]{1,2,0:T(2,128)} %get-tuple-element.24) | copy-start | bytes 388
  147.5 21.3 %all-to-all-start.4 = ((bf16[64,2,512]{2,1,0:T(2,128)(2,1)}), bf16[64,2,512]{2,1,0:T(2,128)(2,1)S(1)}, u32[]{:S(2)}, u32[]{:S(2)}) async-start(bf16[64,2,512]{2,1,0:T(2,128)(2,1)} %reshape.118), calls=%async_computation.4 | async-start | bytes 262144 | tf_op jit(solution)/shard_map/all_to_all | solution.py:12
  152.3 0.7 copy-start.9
  153.1 0.7 copy-start.10
  153.8 0.7 copy-start.11
  153.8 0.7 copy-start.12
  167.6 25.4 %copy-start.6 = (bf16[2048,128]{0,1:T(8,128)(2,1)}, bf16[2048,128]{0,1:T(8,128)(2,1)S(1)}, u32[]{:S(2)}) copy-start(bf16[2048,128]{0,1:T(8,128)(2,1)S(1)} %all_gather.7) | copy-start | bytes 1572868
  170.1 0.7 copy-start.17
  173.9 0.6 copy-start.35
  176.0 36.9 %all-to-all-start.5 = ((bf16[64,2,1024]{2,1,0:T(2,128)(2,1)}), bf16[64,2,1024]{2,1,0:T(2,128)(2,1)S(1)}, u32[]{:S(2)}, u32[]{:S(2)}) async-start(bf16[64,2,1024]{2,1,0:T(2,128)(2,1)} %reshape.120), calls=%async_computation.5 | async-start | bytes 524288 | tf_op jit(solution)/shard_map/all_to_all | solution.py:42
  214.3 1.0 copy-start.5
  215.3 0.7 copy-start.16
  218.7 21.9 %all-to-all-start.6 = ((f32[64,1,512]{2,1,0:T(1,128)}), f32[64,1,512]{2,1,0:T(1,128)S(1)}, u32[]{:S(2)}, u32[]{:S(2)}) async-start(f32[64,1,512]{2,1,0:T(1,128)} %reshape.122), calls=%async_computation.6 | async-start | bytes 262144 | tf_op jit(solution)/shard_map/all_to_all | solution.py:12
  242.0 0.9 copy-start.7
  242.0 0.9 copy-start.30
  242.1 0.9 copy-start.36
  242.1 0.9 copy-start.39
  242.3 0.7 copy-start.26
  242.3 0.7 copy-start.27
  242.3 0.7 copy-start.28
  242.3 0.8 copy-start.29
  247.6 4.8 %copy-start.2 = (f32[32,16,2]{2,1,0:T(8,128)S(1)}, f32[32,16,2]{2,1,0:T(8,128)}, u32[]{:S(2)}) copy-start(f32[32,16,2]{2,1,0:T(8,128)} %copy-done.1) | copy-start | bytes 12292
  247.6 4.8 %copy-start.4 = (f32[32,16,128]{2,1,0:T(8,128)S(1)}, f32[32,16,128]{2,1,0:T(8,128)}, u32[]{:S(2)}) copy-start(f32[32,16,128]{2,1,0:T(8,128)} %copy-done.3) | copy-start | bytes 786436
  247.6 26.4 %all-to-all-start.7 = ((f32[64,1,1024]{2,1,0:T(1,128)}), f32[64,1,1024]{2,1,0:T(1,128)S(1)}, u32[]{:S(2)}, u32[]{:S(2)}) async-start(f32[64,1,1024]{2,1,0:T(1,128)} %reshape.124), calls=%async_computation.7 | async-start | bytes 524288 | tf_op jit(solution)/shard_map/all_to_all | solution.py:72
